TPU v7x, 32 devices: a whole 2x2x4 slice. The times are simulated.
32 devices in a mesh: grp: 2 (over y), ep: 4 (over z), tp: 4 (over x, core).
Axes of the slice: x: 2, y: 2, z: 4, core: 2. Of those that a mesh axis runs over, the one named last changes fastest.
Arguments:
- query_rows: bfloat16 [1536, 2048], P(('grp', 'ep'), 'tp'), parts along dimension 0, may hold values from -100 to 100
- projected_keys: bfloat16 [1536, 512], P(('grp', 'ep'), 'tp'), parts along dimension 0, may hold values from -100 to 100
- projected_values: bfloat16 [1536, 512], P(('grp', 'ep'), 'tp'), parts along dimension 0, may hold values from -6 to 6
- query_gain: float32 [128], replicated, may hold values from 0.3 to 6.5
- key_norm_gain: float32 [128], replicated, may hold values from 0.3 to 6.5
- out_proj: bfloat16 [2048, 2048], P('tp'), may hold values from -4 to 4
- mix_tokens: bfloat16 [4096, 2048], P(('grp', 'ep', 'tp')), parts along dimension 0, may hold values from -150 to 150
- norm_gain: float32 [2048], replicated, may hold values from 0.1 to 1.9
- expert_ids: int32 [4096, 2], P(('grp', 'ep', 'tp')), parts along dimension 0, may hold values from 0 to 3, all different within a row; in each aligned block of 128 rows (0 to 127, 128 to 255, ...) at most 96 rows name the same one
- expert_score: float32 [4096, 2], P(('grp', 'ep', 'tp')), parts along dimension 0, may hold values from -6 to 6
- gate_proj: bfloat16 [4, 2048, 2048], P('ep', None, 'tp'), may hold values from -0.125 to 0.125
- up_proj: bfloat16 [4, 2048, 2048], P('ep', None, 'tp'), may hold values from -0.125 to 0.125
- down_proj: bfloat16 [4, 2048, 2048], P('ep', 'tp'), may hold values from -0.125 to 0.125
Outputs:
- mixed_rows: bfloat16 [1536, 2048], P(('grp', 'ep', 'tp')), parts along dimension 0
- expert_out: bfloat16 [4096, 2048], P(('grp', 'ep', 'tp')), parts along dimension 0
There are 2 independent parts, one for each index of `grp`. A program takes and returns all parts, laid end to end along the dimension named above; an argument that names none is the same for every part. Nothing has to cross between parts.
Inputs may be any that keep to these rules, and one draw needn't show every extreme that they name: `expert_ids`: each row names 2 different experts. Within the rows of one device (aligned blocks of 128 rows) no expert is named more than 96 times, and in every draw some device names some expert exactly 96 times.
All inputs are finite; a program needn't handle non-finite values.
Results may differ from a plain program's by a relative error of at most 0.014.
The roundings to bfloat16 on the way count: a program that leaves them out, or rounds other values in their place, can miss the bound.
Values may be sent and summed in bfloat16 or wider, within the bound.
A program may use at most 128 MiB of HBM per device.

v0:
```python
import math
import jax
import jax.numpy as jnp
from jax import lax
from jax.sharding import PartitionSpec as P

GRID_W = 64
EPS = 1e-06
THETA = 10000.0


def head_norm(vectors, gain):
    return vectors * lax.rsqrt(jnp.mean(vectors * vectors, axis=-1, keepdims=True) + EPS) * gain


def rotate_grid(vectors, token_positions):
    length, heads, head_dim = vectors.shape
    quarter = head_dim // 4
    freqs = 1.0 / THETA ** (jnp.arange(quarter, dtype=jnp.float32) * 4.0 / head_dim)
    grid_row = (token_positions // GRID_W).astype(jnp.float32)
    grid_col = (token_positions % GRID_W).astype(jnp.float32)
    angles = jnp.stack([grid_row[:, None] * freqs, grid_col[:, None] * freqs], axis=1)
    cosine = jnp.cos(angles)[:, None]
    sine = jnp.sin(angles)[:, None]
    halves = vectors.reshape(length, heads, 2, 2, quarter)
    first = halves[..., 0, :]
    second = halves[..., 1, :]
    turned = jnp.stack([first * cosine - second * sine, second * cosine + first * sine], axis=-2)
    return turned.reshape(length, heads, head_dim)


def prepare_inputs(raw_rows, gain, heads, token_positions):
    length = raw_rows.shape[0]
    head_dim = gain.shape[0]
    vectors = raw_rows.astype(jnp.float32).reshape(length, heads, head_dim)
    return rotate_grid(head_norm(vectors, gain), token_positions).astype(jnp.bfloat16)


def mixer_half(query_rows, projected_keys, projected_values, query_gain, key_norm_gain, out_proj):
    length = query_rows.shape[0]
    head_dim = query_gain.shape[0]
    kv_heads = projected_keys.shape[1] // head_dim
    q_heads = query_rows.shape[1] // head_dim
    queries_per_group = q_heads // kv_heads
    token_positions = lax.axis_index("ep") * length + jnp.arange(length, dtype=jnp.int32)
    query_matrix = prepare_inputs(query_rows, query_gain, q_heads, token_positions).reshape(
        length, kv_heads, queries_per_group, head_dim
    )
    keys_turned = prepare_inputs(projected_keys, key_norm_gain, kv_heads, token_positions).reshape(
        length, kv_heads * head_dim
    )
    score_scale = head_dim ** (-0.5)
    initial = (
        jnp.full((kv_heads, queries_per_group, length), -1e30, jnp.float32),
        jnp.zeros((kv_heads, queries_per_group, length), jnp.float32),
        jnp.zeros((length, kv_heads, queries_per_group, head_dim), jnp.float32),
    )
    width = kv_heads * head_dim
    pair = lax.all_gather(
        jnp.concatenate([keys_turned, projected_values], axis=1), "ep", axis=0, tiled=True
    )
    key_piece = pair[:, :width]
    value_piece = pair[:, width:]
    piece_rows = key_piece.shape[0]
    step_rows = math.gcd(piece_rows, 1024)

    def one_block(block_index, running):
        run_max, run_sum, run_acc = running
        offset = block_index * step_rows
        key_block = lax.dynamic_slice_in_dim(key_piece, offset, step_rows, 0).reshape(
            step_rows, kv_heads, head_dim
        )
        value_block = lax.dynamic_slice_in_dim(value_piece, offset, step_rows, 0).reshape(
            step_rows, kv_heads, head_dim
        )
        scores = (
            jnp.einsum(
                "tkgd,skd->kgts", query_matrix, key_block, preferred_element_type=jnp.float32
            )
            * score_scale
        )
        new_max = jnp.maximum(run_max, jnp.max(scores, axis=-1))
        factor = jnp.exp(run_max - new_max)
        weights = jnp.exp(scores - new_max[..., None])
        run_sum = run_sum * factor + jnp.sum(weights, axis=-1)
        update = jnp.einsum(
            "kgts,skd->tkgd",
            weights.astype(jnp.bfloat16),
            value_block,
            preferred_element_type=jnp.float32,
        )
        run_acc = run_acc * jnp.transpose(factor, (2, 0, 1))[..., None] + update
        return (new_max, run_sum, run_acc)

    run_max, run_sum, run_acc = lax.fori_loop(0, piece_rows // step_rows, one_block, initial)
    heads_out = (
        (run_acc / jnp.transpose(run_sum, (2, 0, 1))[..., None])
        .astype(jnp.bfloat16)
        .reshape(length, q_heads * head_dim)
    )
    return jnp.dot(heads_out, out_proj, preferred_element_type=jnp.float32).astype(jnp.bfloat16)


def both_halves(
    query_rows,
    projected_keys,
    projected_values,
    query_gain,
    key_norm_gain,
    out_proj,
    mix_tokens,
    norm_gain,
    expert_ids,
    expert_score,
    gate_proj,
    up_proj,
    down_proj,
):
    length, model_dim = mix_tokens.shape
    top_count = expert_ids.shape[1]
    local_experts = gate_proj.shape[0]
    expert_axis = lax.axis_size("ep")
    experts_all = expert_axis * local_experts
    capacity = length * top_count * 3 // (2 * experts_all)
    values_b = mix_tokens.astype(jnp.float32)
    normed = (
        values_b
        * lax.rsqrt(jnp.mean(values_b * values_b, axis=-1, keepdims=True) + EPS)
        * norm_gain
    ).astype(jnp.bfloat16)
    flat = expert_ids.reshape(length * top_count)
    onehot = (flat[:, None] == jnp.arange(experts_all, dtype=jnp.int32)).astype(jnp.int32)
    slots = jnp.sum((jnp.cumsum(onehot, axis=0) - onehot) * onehot, axis=1)
    target = flat * capacity + slots
    placed = (target[:, None] == jnp.arange(experts_all * capacity, dtype=jnp.int32)).astype(
        jnp.int32
    )
    placed = jnp.sum(placed.reshape(length, top_count, experts_all * capacity), axis=1).astype(
        jnp.bfloat16
    )
    outgoing = jnp.einsum("re,rd->ed", placed, normed, preferred_element_type=jnp.float32).astype(
        jnp.bfloat16
    )
    outgoing = outgoing.reshape(expert_axis, local_experts, capacity, model_dim)
    arrived = lax.all_to_all(outgoing, "ep", split_axis=0, concat_axis=0, tiled=True)
    arrived, query_rows, projected_keys, projected_values = lax.optimization_barrier(
        (arrived, query_rows, projected_keys, projected_values)
    )
    rows_in = lax.all_gather(arrived, "tp", axis=0, tiled=True)
    head_partial = mixer_half(
        query_rows, projected_keys, projected_values, query_gain, key_norm_gain, out_proj
    )
    rows_in, head_partial = lax.optimization_barrier((rows_in, head_partial))
    mixed_rows = lax.psum_scatter(head_partial, "tp", scatter_dimension=0, tiled=True)
    gate_out = jnp.einsum("secd,edf->secf", rows_in, gate_proj, preferred_element_type=jnp.float32)
    up_out = jnp.einsum("secd,edf->secf", rows_in, up_proj, preferred_element_type=jnp.float32)
    active = (jax.nn.silu(gate_out) * up_out).astype(jnp.bfloat16)
    summed = lax.psum_scatter(
        jnp.einsum("secf,efd->secd", active, down_proj, preferred_element_type=jnp.float32).astype(
            jnp.bfloat16
        ),
        "tp",
        scatter_dimension=0,
        tiled=True,
    )
    returned = lax.all_to_all(summed, "ep", split_axis=0, concat_axis=0, tiled=True)
    results = returned.reshape(experts_all * capacity, model_dim)
    first_weight = jax.nn.sigmoid(expert_score[:, 0] - expert_score[:, 1])
    picks = target.reshape(length, top_count)
    chosen = [
        jnp.dot(
            (picks[:, k : k + 1] == jnp.arange(experts_all * capacity, dtype=jnp.int32)).astype(
                jnp.bfloat16
            ),
            results,
            preferred_element_type=jnp.float32,
        )
        for k in range(2)
    ]
    combined = first_weight[:, None] * chosen[0] + (1.0 - first_weight)[:, None] * chosen[1]
    return (mixed_rows, combined.astype(jnp.bfloat16))


def local(
    query_rows,
    projected_keys,
    projected_values,
    query_gain,
    key_norm_gain,
    out_proj,
    mix_tokens,
    norm_gain,
    expert_ids,
    expert_score,
    gate_proj,
    up_proj,
    down_proj,
):
    return both_halves(
        query_rows,
        projected_keys,
        projected_values,
        query_gain,
        key_norm_gain,
        out_proj,
        mix_tokens,
        norm_gain,
        expert_ids,
        expert_score,
        gate_proj,
        up_proj,
        down_proj,
    )


def solution(mesh):
    in_specs = (
        P(("grp", "ep"), "tp"),
        P(("grp", "ep"), "tp"),
        P(("grp", "ep"), "tp"),
        P(),
        P(),
        P("tp", None),
        P(("grp", "ep", "tp"), None),
        P(),
        P(("grp", "ep", "tp"), None),
        P(("grp", "ep", "tp"), None),
        P("ep", None, "tp"),
        P("ep", None, "tp"),
        P("ep", "tp", None),
    )
    out_specs = (P(("grp", "ep", "tp"), None), P(("grp", "ep", "tp"), None))
    return jax.shard_map(local, mesh=mesh, in_specs=in_specs, out_specs=out_specs, check_vma=False)
```

profile of v0, /device:TPU:0, one launch (start us, length us, event | category | flops | bytes accessed | tf_op | source)
XLA Modules:
  0.0 235.2 jit_solution(7432642397368163617)
XLA Ops:
  7.2 0.9 copy.77
  8.2 0.1 eq.76
  8.3 0.1 eq.72
  8.4 1.2 fusion.41
  9.7 1.2 reduce-window.6
  11.0 0.1 copy.79
  11.1 0.1 copy.80
  11.3 0.1 reduce_sum.61
  11.5 0.7 multiply_add_fusion
  12.2 0.1 convert_reduce_fusion
  12.3 1.7 convolution_convert_fusion
  14.1 43.3 %all_to_all.10 = bf16[4,1,96,2048]{3,2,1,0:T(8,128)(2,1)} all-to-all(bf16[4,1,96,2048]{3,2,1,0:T(8,128)(2,1)S(1)} %bitcast.177), channel_id=1, replica_groups=mesh['grp'=2,'ep'=4,'tp'=4] {'ep'}, dimensions={0} | all-to-all | bytes 3145728 | tf_op jit(solution)/shard_map/all_to_all | solution.py:145
  57.6 0.1 mul.324
  57.7 0.1 broadcast_multiply_fusion.1
  57.8 0.2 fusion.55
  58.0 0.1 copy.84
  58.2 0.1 copy.83
  58.3 0.1 fusion.50
  58.4 0.3 subtract_convert_fusion.1
  58.7 0.1 copy.85
  58.8 0.1 copy.86
  59.1 0.1 multiply_multiply_fusion
  59.2 0.1 subtract_convert_fusion
  59.3 0.2 copy.87
  59.5 15.1 %all_gather.7 = bf16[768,256]{1,0:T(8,128)(2,1)S(1)} all-gather(bf16[192,256]{1,0:T(8,128)(2,1)S(1)} %copy.85), channel_id=1, replica_groups=mesh['grp'=2,'ep'=4,'tp'=4] {'ep'}, dimensions={0}, use_global_device_ids=true | all-gather | bytes 491520 | tf_op jit(solution)/shard_map/all_gather | solution.py:59
  74.6 0.8 fusion.68
  75.3 8.8 %while.18 = (s32[]{:T(128)}, f32[1,4,192]{2,1,0:T(4,128)S(1)}, f32[1,4,192]{2,1,0:T(4,128)S(1)}, f32[192,1,4,128]{3,0,2,1:T(8,128)S(1)}, bf16[768,128]{1,0:T(8,1...) while((s32[]{:T(128)}, f32[1,4,192]{2,1,0:T(4,128)S(1)}, ...), condition=%wide.region_10.11_spmd.clone, body=%wide.region_7.10_spmd.clone.sunk | while | flops 102142472 | bytes 3522743 | solution.py:95
  75.3 1.2 fusion.80
  76.6 0.4 fusion.82
  77.0 1.2 fusion.83
  78.3 1.2 fusion.80
  79.5 0.4 fusion.82
  79.9 1.2 fusion.83
  81.2 1.3 fusion.80
  82.5 0.4 fusion.82
  82.9 1.2 fusion.83
  84.1 0.2 divide_convert_fusion
  84.3 0.2 copy.88
  84.4 3.1 %convolution_convert_fusion.1 = bf16[192,2048]{1,0:T(8,128)(2,1)} fusion(bf16[512,2048]{1,0:T(8,128)(2,1)} %param.20, bf16[24,8,4,128]{3,2,1,0:T(4,128)(2,1)S(1)} %bitcast.183), kind=kOutput, calls=%fused_computation.35 | convolution fusion | flops 403046400 | bytes 3080192 | tf_op jit(solution)/shard_map/dot_general | solution.py:101
  87.5 15.6 %all-gather.2.cloned.1.call-done = bf16[16,1,96,2048]{3,2,1,0:T(8,128)(2,1)} async-done(((bf16[4,1,96,2048]{3,2,1,0:T(8,128)(2,1)}), bf16[16,1,96,2048]{3,2,1,0:T(8,128)(2,1)}) %all-gather.2.cloned.1.call-update) | async-done | bytes 6291472 | tf_op jit(solution)/shard_map/all_gather | solution.py:149
  103.1 8.5 %fusion.15 = f32[16,96,512]{2,1,0:T(8,128)} fusion(bf16[16,1,96,2048]{3,2,1,0:T(8,128)(2,1)} %all-gather.2.cloned.1.call-done, bf16[1,2048,512]{2,1,0:T(8,128)(2,1)} %param.26), kind=kOutput, calls=%fused_computation.22 | convolution fusion | flops 3221225472 | bytes 11534336 | tf_op jit(solution)/shard_map/secd,edf->secf/dot_general | solution.py:156
  111.7 11.9 %convert_bitcast_fusion = bf16[16,1,96,2048]{3,2,0,1:T(8,128)(2,1)} fusion(bf16[1,512,2048]{2,1,0:T(8,128)(2,1)S(1)} %copy-done, f32[16,96,512]{2,1,0:T(8,128)} %fusion.15, bf16[1,2048,512]{2,1,0:T(8,128)(2,1)} %param.25, bf16[16,1,96,2048]{3,2,1,0:T(8,128)(2,1)} %all-gather.2.cloned.1.call-done), kind=kOutput, calls=%fused_computation.26 | convolution fusion | flops 6450315264 | bytes 19922944 | tf_op jit(solution)/shard_map/secf,efd->secd/dot_general | solution.py:159
  123.6 59.0 %reduce-scatter.5.cloned.1.call-done = bf16[4,1,96,2048]{3,2,0,1:T(8,128)(2,1)} async-done(((bf16[16,1,96,2048]{3,2,0,1:T(8,128)(2,1)}), bf16[4,1,96,2048]{3,2,0,1:T(8,128)(2,1)}) %reduce-scatter.5.cloned.1.call-update) | async-done | bytes 1572880 | tf_op jit(solution)/shard_map/reduce_scatter | solution.py:158
  182.6 4.6 %all-to-all-start.1 = ((bf16[4,1,96,2048]{3,2,1,0:T(8,128)(2,1)}), bf16[4,1,96,2048]{3,2,1,0:T(8,128)(2,1)}, u32[]{:S(2)}, u32[]{:S(2)}) async-start(bf16[4,1,96,2048]{3,2,1,0:T(8,128)(2,1)} %bitcast.181), calls=%async_computation.3 | async-start | bytes 3145728 | tf_op jit(solution)/shard_map/all_to_all | solution.py:166
  187.2 0.7 reduce-scatter.3.cloned.1.call-update
  187.9 36.1 %all-to-all-done.1 = bf16[4,1,96,2048]{3,2,1,0:T(8,128)(2,1)} async-done(((bf16[4,1,96,2048]{3,2,1,0:T(8,128)(2,1)}), bf16[4,1,96,2048]{3,2,1,0:T(8,128)(2,1)}, u32[]{:S(2)}, u32[]{:S(2)}) %all-to-all-start.1) | async-done | bytes 1572896 | tf_op jit(solution)/shard_map/all_to_all | solution.py:166
  224.1 1.9 convolution_multiply_fusion.2
  226.0 2.7 %fusion.24 = bf16[128,2048]{1,0:T(8,128)(2,1)} fusion(f32[128,2048]{1,0:T(8,128)S(1)} %convolution_multiply_fusion.2, bf16[384,2048]{1,0:T(8,128)(2,1)} %bitcast.35, f32[128]{0:T(128)S(1)} %get-tuple-element.216, s32[128]{0:T(128)S(1)} %get-tuple-element.232), kind=kOutput, calls=%fused_computation.39 | convolution fusion | flops 202162176 | bytes 3146752 | tf_op jit(solution)/shard_map/dot_general | solution.py:171
  (51 shorter events, 0.8 us)
Async XLA Ops:
  7.2 104.5 %copy-start = (bf16[1,512,2048]{2,1,0:T(8,128)(2,1)S(1)}, bf16[1,512,2048]{2,1,0:T(8,128)(2,1)}, u32[]{:S(2)}) copy-start(bf16[1,512,2048]{2,1,0:T(8,128)(2,1)} %param.27) | copy-start | bytes 6291460
  7.2 96.0 %all-gather.2.cloned.1.call-start = ((), (), s32[]{:S(2)}) async-start(), calls=%async_computation.4 | async-start | bytes 7864320 | tf_op jit(solution)/shard_map/all_gather | solution.py:149
  14.1 43.5 %copy-start.6 = (f32[128]{0:T(128)S(1)}, f32[128]{0:T(128)}, u32[]{:S(2)}) copy-start(f32[128]{0:T(128)} %param.18) | copy-start | bytes 1540
  14.1 43.9 %copy-start.2 = (bf16[192,128]{1,0:T(8,128)(2,1)S(1)}, bf16[192,128]{1,0:T(8,128)(2,1)}, u32[]{:S(2)}) copy-start(bf16[192,128]{1,0:T(8,128)(2,1)} %param.17) | copy-start | bytes 147460
  14.1 44.1 %copy-start.3 = (bf16[192,128]{1,0:T(8,128)(2,1)S(1)}, bf16[192,128]{1,0:T(8,128)(2,1)}, u32[]{:S(2)}) copy-start(bf16[192,128]{1,0:T(8,128)(2,1)} %param.16) | copy-start | bytes 147460
  14.1 44.2 %copy-start.5 = (f32[128]{0:T(128)S(1)}, f32[128]{0:T(128)}, u32[]{:S(2)}) copy-start(f32[128]{0:T(128)} %param.19) | copy-start | bytes 1540
  57.5 1.4 copy-start.1
  57.5 125.1 %reduce-scatter.5.cloned.1.call-start = ((), (), s32[]{:S(2)}) async-start(), calls=%async_computation.6 | async-start | bytes 7864320 | tf_op jit(solution)/shard_map/reduce_scatter | solution.py:158
  123.6 64.3 %copy-start.4 = (f32[128,2]{0,1:T(2,128)S(1)}, f32[128,2]{0,1:T(2,128)}, u32[]{:S(2)}) copy-start(f32[128,2]{0,1:T(2,128)} %param.24) | copy-start | bytes 3076
  182.6 41.5 %all-to-all-start.1 = ((bf16[4,1,96,2048]{3,2,1,0:T(8,128)(2,1)}), bf16[4,1,96,2048]{3,2,1,0:T(8,128)(2,1)}, u32[]{:S(2)}, u32[]{:S(2)}) async-start(bf16[4,1,96,2048]{3,2,1,0:T(8,128)(2,1)} %bitcast.181), calls=%async_computation.3 | async-start | bytes 3145728 | tf_op jit(solution)/shard_map/all_to_all | solution.py:166
  187.2 41.5 %reduce-scatter.3.cloned.1.call-start = ((), (), s32[]{:S(2)}) async-start(), calls=%async_computation.5 | async-start | bytes 983040 | tf_op jit(solution)/shard_map/reduce_scatter | solution.py:154
Sparse Core Ops, SparseCore 0:
  57.6 45.4 all-gather.1
  123.7 58.8 reduce-scatter.4
  191.1 23.7 reduce-scatter.2
where the time goes:
time: 236 us; the launch traced here: 235 us
  waiting for transfers between devices  111 us (47%)
  blocking collectives  58.4 us (25%)
  matrix products  37.2 us (16%)
  between operations  14 us (6%)
  other arithmetic  5.9 us (2%)
  starting transfers between devices  4.68 us (2%)
  local copies, waits for them, and re-layouts  3.36 us (1%)
    reduce_scatter x1, waiting for transfers between devices, both_halves(): lax.psum_scatter(jnp.einsum('secf,efd->secd', active, down_proj, preferre...  59 us
    all_to_all x1, blocking collectives, both_halves(): lax.all_to_all(outgoing, 'ep', split_axis=0, concat_axis=0, tiled=True)  43.3 us
    all_to_all x1, waiting for transfers between devices, both_halves(): lax.all_to_all(summed, 'ep', split_axis=0, concat_axis=0, tiled=True)  36.1 us
    all_gather x1, waiting for transfers between devices, both_halves(): rows_in = lax.all_gather(arrived, 'tp', axis=0, tiled=True)  15.6 us
    all_gather x1, blocking collectives, mixer_half(): lax.all_gather(jnp.concatenate([keys_turned, projected_values], axis=1),...  15.1 us
    dot_general x1, matrix products, both_halves(): jnp.einsum('secf,efd->secd', active, down_proj, preferred_element_type=jn...  11.9 us
    dot_general x1, matrix products, both_halves(): jnp.einsum('secd,edf->secf', rows_in, up_proj, preferred_element_type=jnp...  8.52 us
  transfers between devices with their start and end apart: 4, of which 3 were waited for; matrix products, arithmetic and copies ran while one was open for 8% of the time, Pallas kernels for 0%

commit v1 on v0

--- a/solution.py
+++ b/solution.py
@@ -56,9 +56,11 @@
         jnp.zeros((length, kv_heads, queries_per_group, head_dim), jnp.float32),
     )
     width = kv_heads * head_dim
-    pair = lax.all_gather(
-        jnp.concatenate([keys_turned, projected_values], axis=1), "ep", axis=0, tiled=True
-    )
+    own = jnp.concatenate([keys_turned, projected_values], axis=1)
+    size = lax.axis_size("ep")
+    blocks = jnp.stack([own for _ in range(size)])
+    blocks = lax.all_to_all(blocks, "ep", split_axis=0, concat_axis=0)
+    pair = jnp.concatenate(blocks, axis=0)
     key_piece = pair[:, :width]
     value_piece = pair[:, width:]
     piece_rows = key_piece.shape[0]

time: 236 us -> 236 us (level)
  blocking collectives: 58.4 us -> 43.3 us
  waiting for transfers between devices: 111 us -> 121 us
  starting transfers between devices: 4.68 us -> 8.15 us
    all_gather x1 -> x0, blocking collectives: 15.1 us -> none  [mixer_half(): lax.all_gather(jnp.concatenate([keys_turned, projected_values], axis=1),...]
    all_to_all x0 -> x1, waiting for transfers between devices: none -> 9.19 us  [mixer_half(): blocks = lax.all_to_all(blocks, 'ep', split_axis=0, concat_axis=0)]
    all_to_all x0 -> x1, starting transfers between devices: none -> 3.46 us  [mixer_half(): blocks = lax.all_to_all(blocks, 'ep', split_axis=0, concat_axis=0)]
  transfers between devices with their start and end apart: 4 -> 5, of which waited for: 3 -> 4; matrix products, arithmetic and copies ran while one was open for 8% -> 9% of each run, Pallas kernels for 0% -> 0%
where the time goes in v1:
time: 236 us; the launch traced here: 235 us
  waiting for transfers between devices  121 us (51%)
  blocking collectives  43.3 us (18%)
  matrix products  37.2 us (16%)
  between operations  14.1 us (6%)
  starting transfers between devices  8.15 us (3%)
  other arithmetic  5.9 us (2%)
  local copies, waits for them, and re-layouts  5.07 us (2%)
    reduce_scatter x1, waiting for transfers between devices, both_halves(): lax.psum_scatter(jnp.einsum('secf,efd->secd', active, down_proj, preferre...  59 us
    all_to_all x1, blocking collectives, both_halves(): lax.all_to_all(outgoing, 'ep', split_axis=0, concat_axis=0, tiled=True)  43.3 us
    all_to_all x1, waiting for transfers between devices, both_halves(): lax.all_to_all(summed, 'ep', split_axis=0, concat_axis=0, tiled=True)  36.1 us
    all_gather x1, waiting for transfers between devices, both_halves(): rows_in = lax.all_gather(arrived, 'tp', axis=0, tiled=True)  16.3 us
    dot_general x1, matrix products, both_halves(): jnp.einsum('secf,efd->secd', active, down_proj, preferred_element_type=jn...  11.9 us
    all_to_all x1, waiting for transfers between devices, mixer_half(): blocks = lax.all_to_all(blocks, 'ep', split_axis=0, concat_axis=0)  9.19 us
    dot_general x1, matrix products, both_halves(): jnp.einsum('secd,edf->secf', rows_in, up_proj, preferred_element_type=jnp...  8.52 us
  transfers between devices with their start and end apart: 5, of which 4 were waited for; matrix products, arithmetic and copies ran while one was open for 9% of the time, Pallas kernels for 0%

profile of v1, /device:TPU:0, one launch (start us, length us, event | category | flops | bytes accessed | tf_op | source)
XLA Modules:
  0.0 235.2 jit_solution(12678971696200661960)
XLA Ops:
  7.2 0.9 copy.75
  8.2 0.1 eq.76
  8.3 0.1 eq.72
  8.4 1.2 fusion.41
  9.7 1.2 reduce-window.6
  11.0 0.1 copy.77
  11.1 0.1 copy.78
  11.3 0.1 reduce_sum.61
  11.5 0.7 multiply_add_fusion
  12.2 0.1 convert_reduce_fusion
  12.3 1.7 convolution_convert_fusion
  14.1 43.3 %all_to_all.15 = bf16[4,1,96,2048]{3,2,1,0:T(8,128)(2,1)} all-to-all(bf16[4,1,96,2048]{3,2,1,0:T(8,128)(2,1)S(1)} %bitcast.178), channel_id=1, replica_groups=mesh['grp'=2,'ep'=4,'tp'=4] {'ep'}, dimensions={0} | all-to-all | bytes 3145728 | tf_op jit(solution)/shard_map/all_to_all | solution.py:147
  57.5 0.1 mul.324
  57.7 0.2 fusion.55
  58.0 0.1 copy.82
  58.1 0.1 copy.81
  58.3 0.1 fusion.50
  58.4 0.3 subtract_convert_fusion.1
  58.7 0.1 copy.83
  58.8 0.8 stack.37
  59.5 3.5 %all-to-all-start.1 = ((bf16[4,192,256]{2,1,0:T(8,128)(2,1)}), bf16[4,192,256]{2,1,0:T(8,128)(2,1)S(1)}, u32[]{:S(2)}, u32[]{:S(2)}) async-start(bf16[4,192,256]{2,1,0:T(8,128)(2,1)} %stack.37), calls=%async_computation.1 | async-start | bytes 786432 | tf_op jit(solution)/shard_map/all_to_all | solution.py:62
  63.1 1.1 copy.84
  64.3 0.1 multiply_multiply_fusion
  64.5 0.2 copy.85
  64.7 9.2 %all-to-all-done.1 = bf16[4,192,256]{2,1,0:T(8,128)(2,1)S(1)} async-done(((bf16[4,192,256]{2,1,0:T(8,128)(2,1)}), bf16[4,192,256]{2,1,0:T(8,128)(2,1)S(1)}, u32[]{:S(2)}, u32[]{:S(2)}) %all-to-all-start.1) | async-done | bytes 393248 | tf_op jit(solution)/shard_map/all_to_all | solution.py:62
  73.9 0.8 fusion.68
  74.6 8.8 %while.18 = (s32[]{:T(128)}, f32[1,4,192]{2,1,0:T(4,128)S(1)}, f32[1,4,192]{2,1,0:T(4,128)S(1)}, f32[192,1,4,128]{3,0,2,1:T(8,128)S(1)}, bf16[768,128]{1,0:T(8,1...) while((s32[]{:T(128)}, f32[1,4,192]{2,1,0:T(4,128)S(1)}, ...), condition=%wide.region_10.11_spmd.clone, body=%wide.region_7.10_spmd.clone.sunk | while | flops 102142472 | bytes 3522743 | solution.py:97
  74.6 1.2 fusion.80
  75.9 0.4 fusion.82
  76.3 1.2 fusion.83
  77.5 1.2 fusion.80
  78.8 0.4 fusion.82
  79.2 1.2 fusion.83
  80.5 1.3 fusion.80
  81.7 0.4 fusion.82
  82.2 1.2 fusion.83
  83.4 0.2 divide_convert_fusion
  83.6 0.2 copy.86
  83.7 3.1 %convolution_convert_fusion.1 = bf16[192,2048]{1,0:T(8,128)(2,1)} fusion(bf16[512,2048]{1,0:T(8,128)(2,1)} %param.20, bf16[24,8,4,128]{3,2,1,0:T(4,128)(2,1)S(1)} %bitcast.185), kind=kOutput, calls=%fused_computation.35 | convolution fusion | flops 403046400 | bytes 3080192 | tf_op jit(solution)/shard_map/dot_general | solution.py:103
  86.8 16.3 %all-gather.2.cloned.1.call-done = bf16[16,1,96,2048]{3,2,1,0:T(8,128)(2,1)} async-done(((bf16[4,1,96,2048]{3,2,1,0:T(8,128)(2,1)}), bf16[16,1,96,2048]{3,2,1,0:T(8,128)(2,1)}) %all-gather.2.cloned.1.call-update) | async-done | bytes 6291472 | tf_op jit(solution)/shard_map/all_gather | solution.py:151
  103.2 8.5 %fusion.15 = f32[16,96,512]{2,1,0:T(8,128)} fusion(bf16[16,1,96,2048]{3,2,1,0:T(8,128)(2,1)} %all-gather.2.cloned.1.call-done, bf16[1,2048,512]{2,1,0:T(8,128)(2,1)} %param.26), kind=kOutput, calls=%fused_computation.22 | convolution fusion | flops 3221225472 | bytes 11534336 | tf_op jit(solution)/shard_map/secd,edf->secf/dot_general | solution.py:158
  111.7 11.9 %convert_bitcast_fusion = bf16[16,1,96,2048]{3,2,0,1:T(8,128)(2,1)} fusion(bf16[1,512,2048]{2,1,0:T(8,128)(2,1)S(1)} %copy-done, f32[16,96,512]{2,1,0:T(8,128)} %fusion.15, bf16[1,2048,512]{2,1,0:T(8,128)(2,1)} %param.25, bf16[16,1,96,2048]{3,2,1,0:T(8,128)(2,1)} %all-gather.2.cloned.1.call-done), kind=kOutput, calls=%fused_computation.26 | convolution fusion | flops 6450315264 | bytes 19922944 | tf_op jit(solution)/shard_map/secf,efd->secd/dot_general | solution.py:161
  123.6 59.0 %reduce-scatter.5.cloned.1.call-done = bf16[4,1,96,2048]{3,2,0,1:T(8,128)(2,1)} async-done(((bf16[16,1,96,2048]{3,2,0,1:T(8,128)(2,1)}), bf16[4,1,96,2048]{3,2,0,1:T(8,128)(2,1)}) %reduce-scatter.5.cloned.1.call-update) | async-done | bytes 1572880 | tf_op jit(solution)/shard_map/reduce_scatter | solution.py:160
  182.6 4.6 %all-to-all-start.2 = ((bf16[4,1,96,2048]{3,2,1,0:T(8,128)(2,1)}), bf16[4,1,96,2048]{3,2,1,0:T(8,128)(2,1)}, u32[]{:S(2)}, u32[]{:S(2)}) async-start(bf16[4,1,96,2048]{3,2,1,0:T(8,128)(2,1)} %bitcast.182), calls=%async_computation.4 | async-start | bytes 3145728 | tf_op jit(solution)/shard_map/all_to_all | solution.py:168
  187.2 0.7 reduce-scatter.3.cloned.1.call-update
  188.0 36.1 %all-to-all-done.2 = bf16[4,1,96,2048]{3,2,1,0:T(8,128)(2,1)} async-done(((bf16[4,1,96,2048]{3,2,1,0:T(8,128)(2,1)}), bf16[4,1,96,2048]{3,2,1,0:T(8,128)(2,1)}, u32[]{:S(2)}, u32[]{:S(2)}) %all-to-all-start.2) | async-done | bytes 1572896 | tf_op jit(solution)/shard_map/all_to_all | solution.py:168
  224.1 1.9 convolution_multiply_fusion.2
  226.0 2.7 %fusion.24 = bf16[128,2048]{1,0:T(8,128)(2,1)} fusion(f32[128,2048]{1,0:T(8,128)S(1)} %convolution_multiply_fusion.2, bf16[384,2048]{1,0:T(8,128)(2,1)} %bitcast.36, f32[128]{0:T(128)S(1)} %get-tuple-element.216, s32[128]{0:T(128)S(1)} %get-tuple-element.232), kind=kOutput, calls=%fused_computation.39 | convolution fusion | flops 202162176 | bytes 3146752 | tf_op jit(solution)/shard_map/dot_general | solution.py:173
  (51 shorter events, 0.9 us)
Async XLA Ops:
  7.2 104.5 %copy-start = (bf16[1,512,2048]{2,1,0:T(8,128)(2,1)S(1)}, bf16[1,512,2048]{2,1,0:T(8,128)(2,1)}, u32[]{:S(2)}) copy-start(bf16[1,512,2048]{2,1,0:T(8,128)(2,1)} %param.27) | copy-start | bytes 6291460
  7.2 96.0 %all-gather.2.cloned.1.call-start = ((), (), s32[]{:S(2)}) async-start(), calls=%async_computation.5 | async-start | bytes 7864320 | tf_op jit(solution)/shard_map/all_gather | solution.py:151
  14.1 43.5 %copy-start.5 = (f32[128]{0:T(128)S(1)}, f32[128]{0:T(128)}, u32[]{:S(2)}) copy-start(f32[128]{0:T(128)} %param.18) | copy-start | bytes 1540
  14.1 43.9 %copy-start.1 = (bf16[192,128]{1,0:T(8,128)(2,1)S(1)}, bf16[192,128]{1,0:T(8,128)(2,1)}, u32[]{:S(2)}) copy-start(bf16[192,128]{1,0:T(8,128)(2,1)} %param.17) | copy-start | bytes 147460
  14.1 44.0 %copy-start.2 = (bf16[192,128]{1,0:T(8,128)(2,1)S(1)}, bf16[192,128]{1,0:T(8,128)(2,1)}, u32[]{:S(2)}) copy-start(bf16[192,128]{1,0:T(8,128)(2,1)} %param.16) | copy-start | bytes 147460
  14.1 44.2 %copy-start.4 = (f32[128]{0:T(128)S(1)}, f32[128]{0:T(128)}, u32[]{:S(2)}) copy-start(f32[128]{0:T(128)} %param.19) | copy-start | bytes 1540
  59.5 14.3 %all-to-all-start.1 = ((bf16[4,192,256]{2,1,0:T(8,128)(2,1)}), bf16[4,192,256]{2,1,0:T(8,128)(2,1)S(1)}, u32[]{:S(2)}, u32[]{:S(2)}) async-start(bf16[4,192,256]{2,1,0:T(8,128)(2,1)} %stack.37), calls=%async_computation.1 | async-start | bytes 786432 | tf_op jit(solution)/shard_map/all_to_all | solution.py:62
  63.0 119.6 %reduce-scatter.5.cloned.1.call-start = ((), (), s32[]{:S(2)}) async-start(), calls=%async_computation.7 | async-start | bytes 7864320 | tf_op jit(solution)/shard_map/reduce_scatter | solution.py:160
  123.6 64.3 %copy-start.3 = (f32[128,2]{0,1:T(2,128)S(1)}, f32[128,2]{0,1:T(2,128)}, u32[]{:S(2)}) copy-start(f32[128,2]{0,1:T(2,128)} %param.24) | copy-start | bytes 3076
  182.6 41.5 %all-to-all-start.2 = ((bf16[4,1,96,2048]{3,2,1,0:T(8,128)(2,1)}), bf16[4,1,96,2048]{3,2,1,0:T(8,128)(2,1)}, u32[]{:S(2)}, u32[]{:S(2)}) async-start(bf16[4,1,96,2048]{3,2,1,0:T(8,128)(2,1)} %bitcast.182), calls=%async_computation.4 | async-start | bytes 3145728 | tf_op jit(solution)/shard_map/all_to_all | solution.py:168
  187.2 41.5 %reduce-scatter.3.cloned.1.call-start = ((), (), s32[]{:S(2)}) async-start(), calls=%async_computation.6 | async-start | bytes 983040 | tf_op jit(solution)/shard_map/reduce_scatter | solution.py:156
Sparse Core Ops, SparseCore 0:
  57.6 45.5 all-gather.1
  123.7 58.8 reduce-scatter.4
  191.1 23.7 reduce-scatter.2
